TPU v7x, 32 devices: a whole 2x2x4 slice. The times are simulated.
32 devices in a mesh: rep: 2 (over x), fs: 8 (over z, y), tp: 2 (over core).
Axes of the slice: x: 2, y: 2, z: 4, core: 2. Of those that a mesh axis runs over, the one named last changes fastest.
Arguments:
- activations: bfloat16 [3072, 2048], P(('rep', 'fs'), 'tp'), may hold values from -6 to 6
- mix_gain: float32 [2048], replicated, may hold values from 0.1 to 1.9
- mlp_gain: float32 [2048], replicated, may hold values from 0.1 to 1.9
- query_weight: float32 [2048, 512], P('fs', 'tp'), may hold values from -0.125 to 0.125
- query_scale: float32 [512], P('tp'), may hold values from 0.3 to 3
- key_weight: float32 [2048, 512], P('fs', 'tp'), may hold values from -0.125 to 0.125
- key_scale: float32 [512], P('tp'), may hold values from 0.3 to 3
- value_weight: float32 [2048, 1024], P('fs', 'tp'), may hold values from -0.125 to 0.125
- value_scale: float32 [1024], P('tp'), may hold values from 0.3 to 3
- gate_weight: float32 [2048, 1024], P('fs', 'tp'), may hold values from -0.125 to 0.125
- gate_scale: float32 [1024], P('tp'), may hold values from 0.3 to 3
- out_weight: float32 [1024, 2048], P('tp', 'fs'), may hold values from -0.1875 to 0.1875
- out_scale: float32 [2048], P('fs'), may hold values from 0.3 to 3
- up_weight: float32 [2048, 8192], P('fs', 'tp'), may hold values from -0.125 to 0.125
- up_scale: float32 [8192], P('tp'), may hold values from 0.3 to 3
- down_weight: float32 [8192, 2048], P('tp', 'fs'), may hold values from -0.0625 to 0.0625
- down_scale: float32 [2048], P('fs'), may hold values from 0.3 to 3
- log_decay: float32 [8], P('tp'), may hold values from -0.1 to 0, as said below
Outputs:
- result: bfloat16 [3072, 2048], P(('rep', 'fs'), 'tp')
Inputs may be any that keep to these rules, and one draw needn't show every extreme that they name: `log_decay`: negative for every head.
All inputs are finite; a program needn't handle non-finite values.
Results may differ from a plain program's by a relative error of at most 0.023.
Values may be sent and summed in bfloat16 or wider, within the bound.
A program may use at most 128 MiB of HBM per device.

v0:
```python
import jax
import jax.numpy as jnp
from jax import lax
from jax.sharding import PartitionSpec as P

BLOCK = 64
LENGTH = 192
epsilon = 1e-06
rope_base = 10000.0


def rotate(head_rows, positions):
    half = head_rows.shape[-1] // 2
    inverse = 1.0 / rope_base ** jnp.linspace(0.0, 1.0, half, dtype=jnp.float32)
    angles = positions[:, None] * inverse[None, :]
    cosine = jnp.cos(angles)[:, None, :]
    sine = jnp.sin(angles)[:, None, :]
    first = head_rows[..., :half]
    second = head_rows[..., half:]
    return jnp.concatenate(
        [first * cosine - second * sine, first * sine + second * cosine], axis=-1
    )


def retain(query_heads, key_heads, value_heads, log_decay):
    batch, length, heads, width = query_heads.shape
    block_count = length // BLOCK
    highest = lax.Precision.HIGHEST

    def to_blocks(tensor):
        return tensor.reshape(batch, block_count, BLOCK, heads, tensor.shape[-1]).transpose(
            0, 3, 1, 2, 4
        )

    query_blocks = to_blocks(query_heads)
    key_blocks = to_blocks(key_heads)
    value_blocks = to_blocks(value_heads)
    places = jnp.arange(BLOCK, dtype=jnp.float32)
    offsets = places[:, None] - places[None, :]
    inner = jnp.where(
        offsets >= 0, jnp.exp(log_decay[:, None, None] * jnp.maximum(offsets, 0.0)), 0.0
    )
    scores = (
        jnp.einsum("bhntd,bhnsd->bhnts", query_blocks, key_blocks, precision=highest)
        * inner[None, :, None]
    )
    output = jnp.einsum("bhnts,bhnse->bhnte", scores, value_blocks, precision=highest)
    keys_decayed = (
        key_blocks
        * jnp.exp(log_decay[:, None] * (BLOCK - 1.0 - places)[None, :])[None, :, None, :, None]
    )
    increments = jnp.einsum("bhnsd,bhnse->nbhde", keys_decayed, value_blocks, precision=highest)
    carry_decay = jnp.exp(log_decay * BLOCK)[None, :, None, None]

    def advance(state, increment):
        return (carry_decay * state + increment, state)

    initial = jnp.zeros((batch, heads, width, value_heads.shape[-1]), jnp.float32)
    _, states = lax.scan(advance, initial, increments)
    query_decayed = (
        query_blocks * jnp.exp(log_decay[:, None] * (places + 1.0)[None, :])[None, :, None, :, None]
    )
    output = output + jnp.einsum("bhntd,nbhde->bhnte", query_decayed, states, precision=highest)
    return output.transpose(0, 2, 3, 1, 4).reshape(batch, length, heads, value_heads.shape[-1])


def gather_norm(rows, gain):
    whole = lax.all_gather(rows, "tp", axis=1, tiled=True)
    wide = whole.astype(jnp.float32)
    mean_square = jnp.mean(wide * wide, axis=1, keepdims=True)
    return (wide * lax.rsqrt(mean_square + epsilon) * gain).astype(jnp.bfloat16)


def column_terms(weight, scale, hidden):
    partial_value = lax.dot_general(
        weight, hidden, (((0,), (1,)), ((), ())), preferred_element_type=jnp.float32
    )
    return partial_value * scale[:, None]


def on_device(
    activations,
    mix_gain,
    mlp_gain,
    query_weight,
    query_scale,
    key_weight,
    key_scale,
    value_weight,
    value_scale,
    gate_weight,
    gate_scale,
    out_weight,
    out_scale,
    up_weight,
    up_scale,
    down_weight,
    down_scale,
    log_decay,
):
    query_full, key_full, value_full, gate_full, out_full = (
        lax.all_gather(query_weight.astype(jnp.bfloat16), "fs", axis=0, tiled=True),
        lax.all_gather(key_weight.astype(jnp.bfloat16), "fs", axis=0, tiled=True),
        lax.all_gather(value_weight.astype(jnp.bfloat16), "fs", axis=0, tiled=True),
        lax.all_gather(gate_weight.astype(jnp.bfloat16), "fs", axis=0, tiled=True),
        lax.all_gather(out_weight.astype(jnp.bfloat16), "fs", axis=1, tiled=True),
    )
    out_columns, down_columns = (
        lax.all_gather(out_scale, "fs", axis=0, tiled=True),
        lax.all_gather(down_scale, "fs", axis=0, tiled=True),
    )
    normed = gather_norm(activations, mix_gain)
    total_rows = normed.shape[0]
    sequences = total_rows // LENGTH
    heads = log_decay.shape[0]
    query = jnp.dot(normed, query_full, preferred_element_type=jnp.float32) * query_scale
    key_rows = jnp.dot(normed, key_full, preferred_element_type=jnp.float32) * key_scale
    value = jnp.dot(normed, value_full, preferred_element_type=jnp.float32) * value_scale
    gate = jnp.dot(normed, gate_full, preferred_element_type=jnp.float32) * gate_scale
    positions = jnp.arange(LENGTH, dtype=jnp.float32)
    query_heads = rotate(query.reshape(sequences, LENGTH, heads, -1), positions)
    key_heads = rotate(key_rows.reshape(sequences, LENGTH, heads, -1), positions)
    value_heads = value.reshape(sequences, LENGTH, heads, -1)
    retained = retain(query_heads, key_heads, value_heads, log_decay)
    retained = retained * lax.rsqrt(jnp.mean(retained * retained, axis=-1, keepdims=True) + epsilon)
    attended = (retained.reshape(total_rows, -1) * jax.nn.silu(gate)).astype(jnp.bfloat16)
    mixed = lax.psum_scatter(
        column_terms(out_full, out_columns, attended).astype(jnp.bfloat16),
        "tp",
        scatter_dimension=0,
        tiled=True,
    ).astype(jnp.float32)
    first = (activations.astype(jnp.float32) + mixed.T).astype(jnp.bfloat16)
    normed_two = gather_norm(first, mlp_gain)
    up_full, down_full = (
        lax.all_gather(up_weight.astype(jnp.bfloat16), "fs", axis=0, tiled=True),
        lax.all_gather(down_weight.astype(jnp.bfloat16), "fs", axis=1, tiled=True),
    )
    raised = jnp.dot(normed_two, up_full, preferred_element_type=jnp.float32) * up_scale
    hidden = jnp.square(jax.nn.relu(raised)).astype(jnp.bfloat16)
    channel = lax.psum_scatter(
        column_terms(down_full, down_columns, hidden).astype(jnp.bfloat16),
        "tp",
        scatter_dimension=0,
        tiled=True,
    ).astype(jnp.float32)
    return (first.astype(jnp.float32) + channel.T).astype(jnp.bfloat16)


def solution(mesh):
    placed = (
        P(("rep", "fs"), "tp"),
        P(),
        P(),
        P("fs", "tp"),
        P("tp"),
        P("fs", "tp"),
        P("tp"),
        P("fs", "tp"),
        P("tp"),
        P("fs", "tp"),
        P("tp"),
        P("tp", "fs"),
        P("fs"),
        P("fs", "tp"),
        P("tp"),
        P("tp", "fs"),
        P("fs"),
        P("tp"),
    )
    return jax.shard_map(
        on_device, mesh=mesh, in_specs=placed, out_specs=P(("rep", "fs"), "tp"), check_vma=False
    )
```

profile of v0, /device:TPU:0, one launch (start us, length us, event | category | flops | bytes accessed | tf_op | source)
XLA Modules:
  0.0 743.4 jit_solution(15880534284613785428)
XLA Ops:
  6.5 1.7 convert_element_type.68
  10.0 1.8 convert_element_type.70
  13.8 2.5 all_gather.33
  17.0 22.2 %all-gather = f32[8,1,256]{2,1,0:T(1,128)S(1)} all-gather(f32[1,1,256]{2,1,0:T(1,128)S(1)} %bitcast.109), channel_id=1, replica_groups=mesh['rep'=2,'fs'=8,'tp'=2] {'fs'}, dimensions={0}, use_global_device_ids=true | all-gather | bytes 9216 | tf_op jit(solution)/shard_map/all_gather | solution.py:109
  39.2 13.4 %all-gather.10.cloned.1.call-done = bf16[2048,256]{1,0:T(8,128)(2,1)} async-done(((bf16[256,256]{1,0:T(8,128)(2,1)}), bf16[2048,256]{1,0:T(8,128)(2,1)}) %all-gather.10.cloned.1.call-update) | async-done | bytes 1048592 | tf_op jit(solution)/shard_map/all_gather | solution.py:102
  52.6 1.6 convolution_multiply_fusion.7
  54.4 39.3 %all-gather.12.cloned.1.call-done = bf16[2048,256]{1,0:T(8,128)(2,1)} async-done(((bf16[256,256]{1,0:T(8,128)(2,1)}), bf16[2048,256]{1,0:T(8,128)(2,1)}) %all-gather.12.cloned.1.call-update) | async-done | bytes 1048592 | tf_op jit(solution)/shard_map/all_gather | solution.py:103
  93.8 1.6 convolution_multiply_fusion.6
  96.8 46.9 %all-gather.14.cloned.1.call-done = bf16[2048,512]{1,0:T(8,128)(2,1)} async-done(((bf16[256,512]{1,0:T(8,128)(2,1)}), bf16[2048,512]{1,0:T(8,128)(2,1)}) %all-gather.14.cloned.1.call-update) | async-done | bytes 2097168 | tf_op jit(solution)/shard_map/all_gather | solution.py:104
  143.7 2.2 convolution_multiply_fusion.4
  147.5 2.3 while.13
  149.9 1.7 multiply_reduce_fusion
  152.0 41.4 %all-gather.16.cloned.1.call-done = bf16[2048,512]{1,0:T(8,128)(2,1)} async-done(((bf16[256,512]{1,0:T(8,128)(2,1)}), bf16[2048,512]{1,0:T(8,128)(2,1)}) %all-gather.16.cloned.1.call-update) | async-done | bytes 2097168 | tf_op jit(solution)/shard_map/all_gather | solution.py:105
  193.4 50.8 %all-gather.18.cloned.1.call-done = bf16[512,2048]{1,0:T(8,128)(2,1)} async-done(((bf16[512,256]{1,0:T(8,128)(2,1)}), bf16[512,2048]{1,0:T(8,128)(2,1)}) %all-gather.18.cloned.1.call-update) | async-done | bytes 2097168 | tf_op jit(solution)/shard_map/all_gather | solution.py:106
  244.4 4.3 fusion.6
  248.8 3.8 convert_element_type.80
  252.7 3.8 convert_element_type.82
  257.2 17.9 %all-gather.1 = f32[8,1,256]{2,1,0:T(1,128)S(1)} all-gather(f32[1,1,256]{2,1,0:T(1,128)S(1)} %bitcast.110), channel_id=1, replica_groups=mesh['rep'=2,'fs'=8,'tp'=2] {'fs'}, dimensions={0}, use_global_device_ids=true | all-gather | bytes 9216 | tf_op jit(solution)/shard_map/all_gather | solution.py:110
  276.3 2.4 all_gather.40
  278.9 207.0 %all-gather.20.cloned.1.call-done = bf16[2048,4096]{1,0:T(8,128)(2,1)} async-done(((bf16[256,4096]{1,0:T(8,128)(2,1)}), bf16[2048,4096]{1,0:T(8,128)(2,1)}) %all-gather.20.cloned.1.call-update) | async-done | bytes 16777232 | tf_op jit(solution)/shard_map/all_gather | solution.py:136
  485.9 227.6 %all-gather.22.cloned.1.call-done = bf16[4096,2048]{1,0:T(8,128)(2,1)} async-done(((bf16[4096,256]{1,0:T(8,128)(2,1)}), bf16[4096,2048]{1,0:T(8,128)(2,1)}) %all-gather.22.cloned.1.call-update) | async-done | bytes 16777232 | tf_op jit(solution)/shard_map/all_gather | solution.py:137
  713.4 15.1 %fusion.5 = bf16[2048,192]{0,1:T(8,128)(2,1)} fusion(bf16[4096,2048]{1,0:T(8,128)(2,1)} %all-gather.22.cloned.1.call-done, f32[2048]{0:T(1024)S(1)} %bitcast.108, bf16[2048,4096]{1,0:T(8,128)(2,1)} %all-gather.20.cloned.1.call-done, f32[4096]{0:T(1024)S(1)} %copy-done.6, bf16[192,2048]{1,0:T(8,128)(2,1)S(1)} %all_gather.40, f32[2048]{0:T(1024)S(1)} %copy-done.8, ...), kind=kOutput, calls=%fused_computation.10 | convolution fusion | flops 6447955968 | bytes 35160832 | tf_op jit(solution)/shard_map/dot_general | solution.py:75
  728.5 6.5 reduce-scatter.5.cloned.1.call-done
  735.0 1.9 fusion.15
  (84 shorter events, 12.4 us)
Async XLA Ops:
  6.5 5.4 copy-start.1
  6.5 6.3 copy-start.2
  6.5 46.1 %all-gather.10.cloned.1.call-start = ((), (), s32[]{:S(2)}) async-start(), calls=%async_computation.2 | async-start | bytes 1179648 | tf_op jit(solution)/shard_map/all_gather | solution.py:102
  8.3 85.5 %all-gather.12.cloned.1.call-start = ((), (), s32[]{:S(2)}) async-start(), calls=%async_computation.3 | async-start | bytes 1179648 | tf_op jit(solution)/shard_map/all_gather | solution.py:103
  10.0 3.8 copy-start
  10.0 133.7 %all-gather.14.cloned.1.call-start = ((), (), s32[]{:S(2)}) async-start(), calls=%async_computation.4 | async-start | bytes 2359296 | tf_op jit(solution)/shard_map/all_gather | solution.py:104
  11.9 181.5 %all-gather.16.cloned.1.call-start = ((), (), s32[]{:S(2)}) async-start(), calls=%async_computation.5 | async-start | bytes 2359296 | tf_op jit(solution)/shard_map/all_gather | solution.py:105
  12.7 4.1 copy-start.3
  12.7 4.3 copy-start.4
  12.8 39.9 %copy-start.7 = (f32[2048]{0:T(1024)S(1)}, f32[2048]{0:T(1024)}, u32[]{:S(2)}) copy-start(f32[2048]{0:T(1024)} %param.23) | copy-start | bytes 24580
  12.8 39.9 %copy-start.11 = (f32[256]{0:T(256)S(1)}, f32[256]{0:T(256)}, u32[]{:S(2)}) copy-start(f32[256]{0:T(256)} %param.26) | copy-start | bytes 3076
  12.8 231.4 %all-gather.18.cloned.1.call-start = ((), (), s32[]{:S(2)}) async-start(), calls=%async_computation.6 | async-start | bytes 2359296 | tf_op jit(solution)/shard_map/all_gather | solution.py:106
  13.6 261.5 %reduce-scatter.3.cloned.1.call-start = ((), (), s32[]{:S(2)}) async-start(), calls=%async_computation.7 | async-start | bytes 1179648 | tf_op jit(solution)/shard_map/reduce_scatter | solution.py:127
  16.9 76.9 %copy-start.12 = (f32[256]{0:T(256)S(1)}, f32[256]{0:T(256)}, u32[]{:S(2)}) copy-start(f32[256]{0:T(256)} %param.28) | copy-start | bytes 3076
  95.7 48.1 %copy-start.9 = (f32[512]{0:T(512)S(1)}, f32[512]{0:T(512)}, u32[]{:S(2)}) copy-start(f32[512]{0:T(512)} %param.30) | copy-start | bytes 6148
  149.8 94.6 %copy-start.10 = (f32[512]{0:T(512)S(1)}, f32[512]{0:T(512)}, u32[]{:S(2)}) copy-start(f32[512]{0:T(512)} %param.32) | copy-start | bytes 6148
  248.8 237.1 %all-gather.20.cloned.1.call-start = ((), (), s32[]{:S(2)}) async-start(), calls=%async_computation.8 | async-start | bytes 18874368 | tf_op jit(solution)/shard_map/all_gather | solution.py:136
  252.6 460.8 %all-gather.22.cloned.1.call-start = ((), (), s32[]{:S(2)}) async-start(), calls=%async_computation.9 | async-start | bytes 18874368 | tf_op jit(solution)/shard_map/all_gather | solution.py:137
  256.5 0.7 copy-start.5
  256.5 478.5 %reduce-scatter.5.cloned.1.call-start = ((), (), s32[]{:S(2)}) async-start(), calls=%async_computation.10 | async-start | bytes 1179648 | tf_op jit(solution)/shard_map/reduce_scatter | solution.py:141
  275.1 438.3 %copy-start.6 = (f32[4096]{0:T(1024)S(1)}, f32[4096]{0:T(1024)}, u32[]{:S(2)}) copy-start(f32[4096]{0:T(1024)} %param.36) | copy-start | bytes 49156
  275.1 438.3 %copy-start.8 = (f32[2048]{0:T(1024)S(1)}, f32[2048]{0:T(1024)}, u32[]{:S(2)}) copy-start(f32[2048]{0:T(1024)} %param.24) | copy-start | bytes 24580
Sparse Core Ops, SparseCore 0:
  9.5 43.1 all-gather.9
  54.7 38.9 all-gather.11
  95.9 47.7 all-gather.13
  145.7 47.6 all-gather.15
  195.2 48.8 all-gather.17
  248.9 6.3 reduce-scatter.2
  257.4 228.4 all-gather.19
  487.9 225.4 all-gather.21
  728.6 6.3 reduce-scatter.4
where the time goes:
time: 744 us; the launch traced here: 743 us
  waiting for transfers between devices  633 us (85%)
  blocking collectives  45 us (6%)
  matrix products  28.8 us (4%)
  other arithmetic  20.7 us (3%)
  between operations  13.5 us (2%)
    all_gather x1, waiting for transfers between devices, on_device(): lax.all_gather(down_weight.astype(jnp.bfloat16), 'fs', axis=1, tiled=True)  228 us
    all_gather x1, waiting for transfers between devices, on_device(): lax.all_gather(up_weight.astype(jnp.bfloat16), 'fs', axis=0, tiled=True)  207 us
    all_gather x1, waiting for transfers between devices, on_device(): lax.all_gather(out_weight.astype(jnp.bfloat16), 'fs', axis=1, tiled=True)  50.8 us
    all_gather x1, waiting for transfers between devices, on_device(): lax.all_gather(value_weight.astype(jnp.bfloat16), 'fs', axis=0, tiled=True)  46.9 us
    all_gather x1, waiting for transfers between devices, on_device(): lax.all_gather(gate_weight.astype(jnp.bfloat16), 'fs', axis=0, tiled=True)  41.4 us
    all_gather x1, waiting for transfers between devices, on_device(): lax.all_gather(key_weight.astype(jnp.bfloat16), 'fs', axis=0, tiled=True)  39.3 us
    all_gather x1, blocking collectives, on_device(): lax.all_gather(out_scale, 'fs', axis=0, tiled=True)  22.2 us
    dot_general x2, matrix products, column_terms(): lax.dot_general(weight, hidden, (((0,), (1,)), ((), ())), preferred_eleme...  19.4 us
  transfers between devices with their start and end apart: 9, of which 8 were waited for; matrix products, arithmetic and copies ran while one was open for 4% of the time, Pallas kernels for 0%

commit v1 on v0

--- a/solution.py
+++ b/solution.py
@@ -132,9 +132,15 @@
     ).astype(jnp.float32)
     first = (activations.astype(jnp.float32) + mixed.T).astype(jnp.bfloat16)
     normed_two = gather_norm(first, mlp_gain)
+
+    def prepare_layers_all_on_mesh(array_here):
+        r1 = jax.lax.all_gather(array_here, "fs")
+        next_value = jnp.concatenate(r1, axis=1)
+        return next_value
+
     up_full, down_full = (
         lax.all_gather(up_weight.astype(jnp.bfloat16), "fs", axis=0, tiled=True),
-        lax.all_gather(down_weight.astype(jnp.bfloat16), "fs", axis=1, tiled=True),
+        prepare_layers_all_on_mesh(down_weight.astype(jnp.bfloat16)),
     )
     raised = jnp.dot(normed_two, up_full, preferred_element_type=jnp.float32) * up_scale
     hidden = jnp.square(jax.nn.relu(raised)).astype(jnp.bfloat16)

time: 744 us -> 746 us (level)
  waiting for transfers between devices: 633 us -> 610 us
  local copies, waits for them, and re-layouts: 2.06 us -> 23.3 us
    reshape x0 -> x1, local copies, waits for them, and re-layouts: none -> 21.2 us  [prepare_layers_all_on_mesh(): next_value = jnp.concatenate(r1, axis=1)]
    all_gather x1, waiting for transfers between devices: 228 us -> 207 us  [prepare_layers_all_on_mesh(): r1 = jax.lax.all_gather(array_here, 'fs')]
  transfers between devices with their start and end apart: 9 -> 9, of which waited for: 8 -> 8; matrix products, arithmetic and copies ran while one was open for 4% -> 7% of each run, Pallas kernels for 0% -> 0%
where the time goes in v1:
time: 746 us; the launch traced here: 745 us
  waiting for transfers between devices  610 us (82%)
  blocking collectives  45.3 us (6%)
  matrix products  31.6 us (4%)
  local copies, waits for them, and re-layouts  23.3 us (3%)
  other arithmetic  20.5 us (3%)
  between operations  13.5 us (2%)
    all_gather x1, waiting for transfers between devices, prepare_layers_all_on_mesh(): r1 = jax.lax.all_gather(array_here, 'fs')  207 us
    all_gather x1, waiting for transfers between devices, on_device(): lax.all_gather(up_weight.astype(jnp.bfloat16), 'fs', axis=0, tiled=True)  206 us
    all_gather x1, waiting for transfers between devices, on_device(): lax.all_gather(out_weight.astype(jnp.bfloat16), 'fs', axis=1, tiled=True)  50.8 us
    all_gather x1, waiting for transfers between devices, on_device(): lax.all_gather(value_weight.astype(jnp.bfloat16), 'fs', axis=0, tiled=True)  46.1 us
    all_gather x1, waiting for transfers between devices, on_device(): lax.all_gather(gate_weight.astype(jnp.bfloat16), 'fs', axis=0, tiled=True)  40.4 us
    all_gather x1, waiting for transfers between devices, on_device(): lax.all_gather(key_weight.astype(jnp.bfloat16), 'fs', axis=0, tiled=True)  39.3 us
    all_gather x1, blocking collectives, on_device(): lax.all_gather(out_scale, 'fs', axis=0, tiled=True)  22.2 us
    reshape x1, local copies, waits for them, and re-layouts, prepare_layers_all_on_mesh(): next_value = jnp.concatenate(r1, axis=1)  21.2 us
  transfers between devices with their start and end apart: 9, of which 8 were waited for; matrix products, arithmetic and copies ran while one was open for 7% of the time, Pallas kernels for 0%

profile of v1, /device:TPU:0, one launch (start us, length us, event | category | flops | bytes accessed | tf_op | source)
XLA Modules:
  0.0 744.5 jit_solution(16678650009503489152)
XLA Ops:
  6.5 1.7 convert_element_type.68
  10.0 1.8 convert_element_type.70
  13.7 2.5 all_gather.36
  16.9 22.2 %all-gather.1 = f32[8,1,256]{2,1,0:T(1,128)S(1)} all-gather(f32[1,1,256]{2,1,0:T(1,128)S(1)} %bitcast.115), channel_id=1, replica_groups=mesh['rep'=2,'fs'=8,'tp'=2] {'fs'}, dimensions={0}, use_global_device_ids=true | all-gather | bytes 9216 | tf_op jit(solution)/shard_map/all_gather | solution.py:109
  39.2 13.4 %all-gather.11.cloned.1.call-done = bf16[2048,256]{1,0:T(8,128)(2,1)} async-done(((bf16[256,256]{1,0:T(8,128)(2,1)}), bf16[2048,256]{1,0:T(8,128)(2,1)}) %all-gather.11.cloned.1.call-update) | async-done | bytes 1048592 | tf_op jit(solution)/shard_map/all_gather | solution.py:102
  54.4 39.3 %all-gather.13.cloned.1.call-done = bf16[2048,256]{1,0:T(8,128)(2,1)} async-done(((bf16[256,256]{1,0:T(8,128)(2,1)}), bf16[2048,256]{1,0:T(8,128)(2,1)}) %all-gather.13.cloned.1.call-update) | async-done | bytes 1048592 | tf_op jit(solution)/shard_map/all_gather | solution.py:103
  93.7 1.6 convolution_multiply_fusion.6
  97.6 46.1 %all-gather.15.cloned.1.call-done = bf16[2048,512]{1,0:T(8,128)(2,1)} async-done(((bf16[256,512]{1,0:T(8,128)(2,1)}), bf16[2048,512]{1,0:T(8,128)(2,1)}) %all-gather.15.cloned.1.call-update) | async-done | bytes 2097168 | tf_op jit(solution)/shard_map/all_gather | solution.py:104
  143.7 2.2 convolution_multiply_fusion.4
  148.5 2.3 while.13
  150.8 1.7 multiply_reduce_fusion
  152.9 40.4 %all-gather.17.cloned.1.call-done = bf16[2048,512]{1,0:T(8,128)(2,1)} async-done(((bf16[256,512]{1,0:T(8,128)(2,1)}), bf16[2048,512]{1,0:T(8,128)(2,1)}) %all-gather.17.cloned.1.call-update) | async-done | bytes 2097168 | tf_op jit(solution)/shard_map/all_gather | solution.py:105
  193.3 50.8 %all-gather.19.cloned.1.call-done = bf16[512,2048]{1,0:T(8,128)(2,1)} async-done(((bf16[512,256]{1,0:T(8,128)(2,1)}), bf16[512,2048]{1,0:T(8,128)(2,1)}) %all-gather.19.cloned.1.call-update) | async-done | bytes 2097168 | tf_op jit(solution)/shard_map/all_gather | solution.py:106
  244.4 4.3 fusion.6
  248.8 3.7 convert_element_type.82
  252.6 3.9 convert_element_type.80
  257.1 18.0 %all-gather.2 = f32[8,1,256]{2,1,0:T(1,128)S(1)} all-gather(f32[1,1,256]{2,1,0:T(1,128)S(1)} %bitcast.116), channel_id=1, replica_groups=mesh['rep'=2,'fs'=8,'tp'=2] {'fs'}, dimensions={0}, use_global_device_ids=true | all-gather | bytes 9216 | tf_op jit(solution)/shard_map/all_gather | solution.py:110
  276.2 2.5 all_gather.43
  279.0 206.8 %all-gather.23.cloned.1.call-done = bf16[32768,256]{1,0:T(8,128)(2,1)} async-done(((bf16[4096,256]{1,0:T(8,128)(2,1)}), bf16[32768,256]{1,0:T(8,128)(2,1)}) %all-gather.23.cloned.1.call-update) | async-done | bytes 16777232 | tf_op jit(solution)/shard_map/all_gather | solution.py:137
  485.8 21.2 %copy.68 = bf16[4096,8,256]{0,2,1:T(8,128)(2,1)} copy(bf16[4096,8,256]{2,0,1:T(8,128)(2,1)} %bitcast.101) | data formatting | bytes 33554432 | tf_op jit(solution)/shard_map/reshape | solution.py:138
  507.0 206.4 %all-gather.21.cloned.1.call-done = bf16[2048,4096]{1,0:T(8,128)(2,1)} async-done(((bf16[256,4096]{1,0:T(8,128)(2,1)}), bf16[2048,4096]{1,0:T(8,128)(2,1)}) %all-gather.21.cloned.1.call-update) | async-done | bytes 16777232 | tf_op jit(solution)/shard_map/all_gather | solution.py:142
  713.4 16.2 %fusion.5 = bf16[2048,192]{0,1:T(8,128)(2,1)} fusion(bf16[4096,2048]{0,1:T(8,128)(2,1)} %bitcast.102, f32[2048]{0:T(1024)S(1)} %bitcast.114, bf16[2048,4096]{1,0:T(8,128)(2,1)} %all-gather.21.cloned.1.call-done, f32[4096]{0:T(1024)S(1)} %copy-done.6, bf16[192,2048]{1,0:T(8,128)(2,1)S(1)} %all_gather.43, f32[2048]{0:T(1024)S(1)} %copy-done.8, ...), kind=kOutput, calls=%fused_computation.10 | convolution fusion | flops 6447955968 | bytes 35160832 | tf_op jit(solution)/shard_map/dot_general | solution.py:75
  729.6 6.5 reduce-scatter.5.cloned.1.call-done
  736.1 1.9 fusion.15
  (85 shorter events, 15.7 us)
Async XLA Ops:
  6.5 5.4 copy-start.1
  6.5 6.3 copy-start.2
  6.5 46.1 %all-gather.11.cloned.1.call-start = ((), (), s32[]{:S(2)}) async-start(), calls=%async_computation.2 | async-start | bytes 1179648 | tf_op jit(solution)/shard_map/all_gather | solution.py:102
  8.3 85.5 %all-gather.13.cloned.1.call-start = ((), (), s32[]{:S(2)}) async-start(), calls=%async_computation.3 | async-start | bytes 1179648 | tf_op jit(solution)/shard_map/all_gather | solution.py:103
  10.0 3.7 copy-start
  10.0 133.7 %all-gather.15.cloned.1.call-start = ((), (), s32[]{:S(2)}) async-start(), calls=%async_computation.4 | async-start | bytes 2359296 | tf_op jit(solution)/shard_map/all_gather | solution.py:104
  11.9 181.5 %all-gather.17.cloned.1.call-start = ((), (), s32[]{:S(2)}) async-start(), calls=%async_computation.5 | async-start | bytes 2359296 | tf_op jit(solution)/shard_map/all_gather | solution.py:105
  12.7 4.0 copy-start.3
  12.7 4.2 copy-start.4
  12.7 39.9 %copy-start.7 = (f32[2048]{0:T(1024)S(1)}, f32[2048]{0:T(1024)}, u32[]{:S(2)}) copy-start(f32[2048]{0:T(1024)} %param.23) | copy-start | bytes 24580
  12.7 39.9 %copy-start.11 = (f32[256]{0:T(256)S(1)}, f32[256]{0:T(256)}, u32[]{:S(2)}) copy-start(f32[256]{0:T(256)} %param.26) | copy-start | bytes 3076
  12.7 231.4 %all-gather.19.cloned.1.call-start = ((), (), s32[]{:S(2)}) async-start(), calls=%async_computation.6 | async-start | bytes 2359296 | tf_op jit(solution)/shard_map/all_gather | solution.py:106
  13.6 261.6 %reduce-scatter.3.cloned.1.call-start = ((), (), s32[]{:S(2)}) async-start(), calls=%async_computation.7 | async-start | bytes 1179648 | tf_op jit(solution)/shard_map/reduce_scatter | solution.py:127
  16.7 77.0 %copy-start.12 = (f32[256]{0:T(256)S(1)}, f32[256]{0:T(256)}, u32[]{:S(2)}) copy-start(f32[256]{0:T(256)} %param.28) | copy-start | bytes 3076
  95.7 48.1 %copy-start.9 = (f32[512]{0:T(512)S(1)}, f32[512]{0:T(512)}, u32[]{:S(2)}) copy-start(f32[512]{0:T(512)} %param.30) | copy-start | bytes 6148
  150.8 93.6 %copy-start.10 = (f32[512]{0:T(512)S(1)}, f32[512]{0:T(512)}, u32[]{:S(2)}) copy-start(f32[512]{0:T(512)} %param.32) | copy-start | bytes 6148
  248.7 237.1 %all-gather.23.cloned.1.call-start = ((), (), s32[]{:S(2)}) async-start(), calls=%async_computation.10 | async-start | bytes 18874368 | tf_op jit(solution)/shard_map/all_gather | solution.py:137
  252.5 460.9 %all-gather.21.cloned.1.call-start = ((), (), s32[]{:S(2)}) async-start(), calls=%async_computation.8 | async-start | bytes 18874368 | tf_op jit(solution)/shard_map/all_gather | solution.py:142
  256.4 0.7 copy-start.5
  256.4 479.7 %reduce-scatter.5.cloned.1.call-start = ((), (), s32[]{:S(2)}) async-start(), calls=%async_computation.9 | async-start | bytes 1179648 | tf_op jit(solution)/shard_map/reduce_scatter | solution.py:147
  485.8 227.6 %copy-start.6 = (f32[4096]{0:T(1024)S(1)}, f32[4096]{0:T(1024)}, u32[]{:S(2)}) copy-start(f32[4096]{0:T(1024)} %param.36) | copy-start | bytes 49156
  485.8 227.6 %copy-start.8 = (f32[2048]{0:T(1024)S(1)}, f32[2048]{0:T(1024)}, u32[]{:S(2)}) copy-start(f32[2048]{0:T(1024)} %param.24) | copy-start | bytes 24580
Sparse Core Ops, SparseCore 0:
  9.5 43.0 all-gather.10
  54.7 38.9 all-gather.12
  95.9 47.7 all-gather.14
  145.7 47.6 all-gather.16
  195.2 48.8 all-gather.18
  248.9 6.3 reduce-scatter.2
  257.4 228.4 all-gather.22
  487.9 225.4 all-gather.20
  729.7 6.3 reduce-scatter.4
